TPU v7x, 32 devices: a whole 2x2x4 slice. The times are simulated.
32 devices in a mesh: sp: 8 (over z, core), tp: 4 (over y, x).
Axes of the slice: x: 2, y: 2, z: 4, core: 2. Of those that a mesh axis runs over, the one named last changes fastest.
Arguments:
- queries: bfloat16 [2048, 1024], P('sp', 'tp'), may hold values from -250 to 250
- keys_values: bfloat16 [2, 2048, 256], P(None, 'sp'), may hold values from -8 to 8
- sink_logits: float32 [16], P('tp'), may hold values from 1 to 5
- proj_weight: bfloat16 [1024, 2048], P('tp'), may hold values from -0.75 to 0.75
- residual: bfloat16 [2048, 2048], P('sp', 'tp'), may hold values from -6 to 6
- norm_gain: float32 [2048], replicated, may hold values from 0.1 to 1.9
- routes: int32 [2048, 2], P('sp'), may hold values from 0 to 7, all different within a row; in each aligned block of 256 rows (0 to 255, 256 to 511, ...) at most 128 rows name the same one
- route_weights: float32 [2048, 2], P('sp'), may hold values from 0.2 to 1
- gate_weight: bfloat16 [8, 2048, 2048], P('sp', None, 'tp'), may hold values from -0.125 to 0.125
- up_weight: bfloat16 [8, 2048, 2048], P('sp', None, 'tp'), may hold values from -0.125 to 0.125
- down_weight: bfloat16 [8, 2048, 2048], P('sp', None, 'tp'), may hold values from -0.125 to 0.125
- shared_gate: bfloat16 [2048, 2048], P(None, 'tp'), may hold values from -0.125 to 0.125
- shared_up: bfloat16 [2048, 2048], P(None, 'tp'), may hold values from -0.125 to 0.125
- shared_down: bfloat16 [2048, 2048], P(None, 'tp'), may hold values from -0.125 to 0.125
Outputs:
- output: bfloat16 [2048, 2048], P('sp', 'tp')
Inputs may be any that keep to these rules, and one draw needn't show every extreme that they name: `routes`: the 2 experts of a position differ. In each aligned block of 256 positions no expert is named by more than 128 positions, and in some block one expert is named by exactly 128.
All inputs are finite; a program needn't handle non-finite values.
Results may differ from a plain program's by a relative error of at most 0.0067.
Values may be sent and summed in bfloat16 or wider, within the bound.
A program may use at most 64 MiB of HBM per device.

v0:
```python
import jax
import jax.numpy as jnp
from jax import lax
from jax.sharding import PartitionSpec as P

D = 2048
HEADS = 16
KV_HEADS = 4
HEAD_WIDTH = 64
WINDOW = 128
TOP_K = 2
EXP_DEV = 1
TOK_DEV = 256
norm_eps = 1e-06


def passed_along(value, axis, steps):
    count = lax.axis_size(axis)
    initial, last = (max(0, -steps), min(count, count - steps))
    return lax.ppermute(value, axis, [(source, source + steps) for source in range(initial, last)])


def per_device(
    queries,
    keys_values,
    sink_logits,
    proj_weight,
    residual,
    norm_gain,
    routes,
    route_weights,
    gate_weight,
    up_weight,
    down_weight,
    shared_gate,
    shared_up,
    shared_down,
):
    tp_index = lax.axis_index("tp")
    sp_index = lax.axis_index("sp")
    sp_count = lax.axis_size("sp")
    tp_count = lax.axis_size("tp")
    heads_here = sink_logits.shape[0]
    col_width = residual.shape[1]
    blocks = TOK_DEV // WINDOW
    kv_group = HEADS // KV_HEADS
    earlier_keys = passed_along(keys_values[:, TOK_DEV - WINDOW :, :], "sp", 1)
    extended = jnp.concatenate([earlier_keys, keys_values], axis=1)
    extended = extended.reshape(2, TOK_DEV + WINDOW, KV_HEADS, HEAD_WIDTH)
    head_ids = tp_index * heads_here + jnp.arange(heads_here, dtype=jnp.int32)
    chosen = jnp.take(extended, head_ids // kv_group, axis=2)
    earlier = chosen[:, :TOK_DEV].reshape(2, blocks, WINDOW, heads_here, HEAD_WIDTH)
    later = chosen[:, WINDOW:].reshape(2, blocks, WINDOW, heads_here, HEAD_WIDTH)
    banded = jnp.concatenate([earlier, later], axis=2)
    query_blocks = queries.reshape(blocks, WINDOW, heads_here, HEAD_WIDTH)
    score_matrix = jnp.einsum(
        "bqhd,bkhd->bhqk", query_blocks, banded[0], preferred_element_type=jnp.float32
    ) * HEAD_WIDTH ** (-0.5)
    query_pos = jnp.arange(WINDOW, dtype=jnp.int32)[:, None]
    key_pos = jnp.arange(2 * WINDOW, dtype=jnp.int32)[None, :]
    distance = WINDOW + query_pos - key_pos
    absolute = (
        sp_index * TOK_DEV
        + jnp.arange(blocks, dtype=jnp.int32)[:, None, None] * WINDOW
        - WINDOW
        + key_pos[None]
    )
    allowed = (distance >= 0)[None] & (distance < WINDOW)[None] & (absolute >= 0)
    masked = jnp.where(allowed[:, None], score_matrix, -jnp.inf)
    sink_value = sink_logits[None, :, None, None]
    highest = jnp.maximum(jnp.max(masked, axis=-1, keepdims=True), sink_value)
    weights_exp = jnp.exp(masked - highest)
    denominator = jnp.sum(weights_exp, axis=-1, keepdims=True) + jnp.exp(sink_value - highest)
    softmax_weights = (weights_exp / denominator).astype(jnp.bfloat16)
    attended_values = jnp.einsum(
        "bhqk,bkhd->bqhd", softmax_weights, banded[1], preferred_element_type=jnp.float32
    )
    attended_values = attended_values.astype(jnp.bfloat16).reshape(TOK_DEV, heads_here * HEAD_WIDTH)
    attended_all = lax.all_gather(attended_values, "tp", axis=1, tiled=True)
    weight_rows = proj_weight.shape[0]
    column_share = lax.all_to_all(
        proj_weight.reshape(weight_rows, tp_count, col_width),
        "tp",
        split_axis=1,
        concat_axis=0,
        tiled=True,
    )
    column_share = column_share.reshape(HEADS * HEAD_WIDTH, col_width)
    feature_sum = jnp.dot(attended_all, column_share, preferred_element_type=jnp.float32)
    stream_cols = (feature_sum + residual.astype(jnp.float32)).astype(jnp.bfloat16)
    stream_rows = lax.all_gather(stream_cols, "tp", axis=1, tiled=True)
    gate_eff = (norm_gain[None, :, None] * gate_weight.astype(jnp.float32)).astype(jnp.bfloat16)
    up_eff = (norm_gain[None, :, None] * up_weight.astype(jnp.float32)).astype(jnp.bfloat16)
    shared_gate_eff = (norm_gain[:, None] * shared_gate.astype(jnp.float32)).astype(jnp.bfloat16)
    shared_up_eff = (norm_gain[:, None] * shared_up.astype(jnp.float32)).astype(jnp.bfloat16)
    experts_total = EXP_DEV * sp_count
    capacity = 2 * TOK_DEV * TOP_K // experts_total
    rows_per_expert = sp_count * capacity
    flat_routes = routes.reshape(-1)
    onehot = (flat_routes[:, None] == jnp.arange(experts_total, dtype=jnp.int32)[None, :]).astype(
        jnp.int32
    )
    before = jnp.cumsum(onehot, axis=0) - onehot
    slot_rank = jnp.sum(before * onehot, axis=1)
    slot_index = (
        flat_routes % EXP_DEV * rows_per_expert + flat_routes // EXP_DEV * capacity + slot_rank
    )
    token_of = jnp.arange(TOK_DEV * TOP_K, dtype=jnp.int32) // TOP_K
    slot_owner = (
        jnp.full((EXP_DEV * rows_per_expert,), TOK_DEV, jnp.int32).at[slot_index].set(token_of)
    )
    picked_rows = jnp.take(stream_rows, slot_owner, axis=0, mode="fill", fill_value=0)
    arrived = lax.all_to_all(
        picked_rows.reshape(EXP_DEV, sp_count, capacity, stream_rows.shape[1]),
        "sp",
        split_axis=1,
        concat_axis=1,
        tiled=True,
    )
    arrived = arrived.reshape(EXP_DEV, rows_per_expert, D)
    routed_squares = jnp.sum(jnp.square(arrived.astype(jnp.float32)), axis=-1)
    gate_sum = jnp.einsum("erd,edf->erf", arrived, gate_eff, preferred_element_type=jnp.float32)
    up_sum = jnp.einsum("erd,edf->erf", arrived, up_eff, preferred_element_type=jnp.float32)
    own_squares = jnp.sum(jnp.square(stream_rows.astype(jnp.float32)), axis=-1)
    shared_gate_sum = jnp.dot(stream_rows, shared_gate_eff, preferred_element_type=jnp.float32)
    shared_up_sum = jnp.dot(stream_rows, shared_up_eff, preferred_element_type=jnp.float32)
    routed_scale = lax.rsqrt(routed_squares / D + norm_eps)[..., None]
    own_scale = lax.rsqrt(own_squares / D + norm_eps)[:, None]
    hidden = (jax.nn.silu(routed_scale * gate_sum) * (routed_scale * up_sum)).astype(jnp.bfloat16)
    shared_hidden = (jax.nn.silu(own_scale * shared_gate_sum) * (own_scale * shared_up_sum)).astype(
        jnp.bfloat16
    )
    routed_piece = lax.all_gather(hidden, "tp", axis=2, tiled=True)
    own_piece = lax.all_gather(shared_hidden[None], "tp", axis=2, tiled=True)
    expert_out = jnp.einsum(
        "erf,efd->erd", routed_piece, down_weight, preferred_element_type=jnp.float32
    )
    shared_out = jnp.dot(own_piece[0], shared_down, preferred_element_type=jnp.float32)
    outgoing = expert_out.astype(jnp.bfloat16).reshape(EXP_DEV, sp_count, capacity, col_width)
    returned = lax.all_to_all(outgoing, "sp", split_axis=1, concat_axis=1, tiled=True).reshape(
        EXP_DEV * rows_per_expert, col_width
    )
    picked = jnp.take(returned, slot_index, axis=0).reshape(TOK_DEV, TOP_K, col_width)
    routed_sum = jnp.einsum("nk,nkd->nd", route_weights, picked.astype(jnp.float32))
    return (stream_cols.astype(jnp.float32) + shared_out + routed_sum).astype(jnp.bfloat16)


def solution(mesh):
    placed = (
        P("sp", "tp"),
        P(None, "sp", None),
        P("tp"),
        P("tp", None),
        P("sp", "tp"),
        P(),
        P("sp", None),
        P("sp", None),
        P("sp", None, "tp"),
        P("sp", None, "tp"),
        P("sp", None, "tp"),
        P(None, "tp"),
        P(None, "tp"),
        P(None, "tp"),
    )
    return jax.shard_map(
        per_device, mesh=mesh, in_specs=placed, out_specs=P("sp", "tp"), check_vma=False
    )
```

profile of v0, /device:TPU:0, one launch (start us, length us, event | category | flops | bytes accessed | tf_op | source)
XLA Modules:
  0.0 293.3 jit_solution(9455327325811044780)
XLA Ops:
  6.5 1.2 copy.63
  7.8 3.2 %collective-permute-start = (bf16[2,128,256]{1,2,0:T(8,128)(2,1)S(1)}, bf16[2,128,256]{1,2,0:T(8,128)(2,1)}, u32[]{:S(2)}, u32[]{:S(2)}) collective-permute-start(bf16[2,128,256]{1,2,0:T(8,128)(2,1)S(1)} %slice.34), channel_id=1, source_target_pairs={{0,4},{4,8},{8,12},{12,16},{16,20},{20,24},{24,28},{1,5},{5,9},{9,... | collective-permute-start | bytes 393224 | tf_op jit(solution)/shard_map/ppermute | solution.py:20
  11.0 2.3 copy.73
  13.3 4.5 %all-to-all-start = ((bf16[256,4,512]{0,2,1:T(8,128)(2,1)}), bf16[256,4,512]{0,2,1:T(8,128)(2,1)S(1)}, u32[]{:S(2)}, u32[]{:S(2)}) async-start(bf16[256,4,512]{0,2,1:T(8,128)(2,1)} %bitcast.91), calls=%async_computation | async-start | bytes 2097152 | tf_op jit(solution)/shard_map/all_to_all | solution.py:81
  18.7 0.9 reshape.384
  19.6 1.0 pad_maximum_fusion
  20.7 1.4 gather_fusion
  22.0 1.1 select_bitcast_fusion
  24.0 1.0 reshape.382
  25.8 1.0 reshape.383
  27.6 1.5 fusion.48
  30.0 12.7 %all_gather.12 = bf16[256,1024]{0,1:T(8,128)(2,1)} all-gather(bf16[256,256]{0,1:T(8,128)(2,1)S(1)} %bitcast.95), channel_id=1, replica_groups=mesh['sp'=8,'tp'=4] {'tp'}, dimensions={1}, use_global_device_ids=true | all-gather | bytes 655360 | tf_op jit(solution)/shard_map/all_gather | solution.py:79
  42.7 1.3 copy.74
  44.0 2.6 fusion.25
  47.1 1.1 reduce-window.6
  48.9 2.4 scatter_custom_fusion
  51.4 20.4 %all-gather.6.cloned.1.call-done = bf16[256,2048]{1,0:T(8,128)(2,1)} async-done(((bf16[256,512]{1,0:T(8,128)(2,1)}), bf16[256,2048]{1,0:T(8,128)(2,1)}) %all-gather.6.cloned.1.call-update) | async-done | bytes 1048592 | tf_op jit(solution)/shard_map/all_gather | solution.py:91
  71.8 10.2 %gather_fusion.1 = bf16[1024,2048]{1,0:T(8,128)(2,1)} fusion(bf16[256,2048]{1,0:T(8,128)(2,1)} %all-gather.6.cloned.1.call-done, s32[1024]{0:T(1024)S(1)} %fusion.39), kind=kCustom, calls=%fused_computation.1 | custom fusion | bytes 8392704 | tf_op jit(solution)/shard_map/jit(_take)/gather | solution.py:112
  82.0 2.5 broadcast_select_fusion
  84.5 98.4 %all_to_all.25 = bf16[1,8,128,2048]{3,2,0,1:T(8,128)(2,1)S(1)} all-to-all(bf16[1,8,128,2048]{3,2,0,1:T(8,128)(2,1)S(1)} %broadcast_select_fusion), channel_id=1, replica_groups=mesh['sp'=8,'tp'=4] {'sp'}, dimensions={1} | all-to-all | bytes 8388608 | tf_op jit(solution)/shard_map/all_to_all | solution.py:113
  182.9 0.9 multiply_reduce_fusion
  184.5 2.4 fusion.3
  186.9 3.7 %multiply_convert_fusion.6 = bf16[1024,512]{1,0:T(8,128)(2,1)} fusion(f32[1024,512]{1,0:T(8,128)S(1)} %fusion.3, bf16[1024,2048]{1,0:T(8,128)(2,1)S(1)} %bitcast.89, bf16[1,2048,512]{2,1,0:T(8,128)(2,1)S(1)} %copy-done.11, f32[2048]{0:T(1024)S(1)} %copy-done.14, f32[1024]{0:T(1024)S(1)} %rsqrt_bitcast_fusion), kind=kOutput, calls=%fused_computation.18 | convolution fusion | flops 2154823680 | bytes 9449472 | tf_op jit(solution)/shard_map/erd,edf->erf/dot_general | solution.py:123
  191.0 50.3 %all-gather.10.cloned.1.call-done = bf16[1024,2048]{1,0:T(8,128)(2,1)} async-done(((bf16[1024,512]{1,0:T(8,128)(2,1)}), bf16[1024,2048]{1,0:T(8,128)(2,1)}) %all-gather.10.cloned.1.call-update) | async-done | bytes 4194320 | tf_op jit(solution)/shard_map/all_gather | solution.py:133
  241.3 5.5 %fusion.16 = bf16[1024,512]{1,0:T(8,128)(2,1)} fusion(bf16[1024,2048]{1,0:T(8,128)(2,1)} %all-gather.10.cloned.1.call-done, bf16[1,2048,512]{2,1,0:T(8,128)(2,1)S(1)} %copy-done), kind=kOutput, calls=%fused_computation.24 | convolution fusion | flops 2148007936 | bytes 7340032 | tf_op jit(solution)/shard_map/erf,efd->erd/dot_general | solution.py:135
  246.8 4.6 %all-to-all-start.2 = ((bf16[1,8,128,512]{3,2,0,1:T(8,128)(2,1)}), bf16[1,8,128,512]{3,2,0,1:T(8,128)(2,1)}, u32[]{:S(2)}, u32[]{:S(2)}) async-start(bf16[1,8,128,512]{3,2,0,1:T(8,128)(2,1)} %bitcast.93), calls=%async_computation.2 | async-start | bytes 2097152 | tf_op jit(solution)/shard_map/all_to_all | solution.py:140
  251.4 2.6 fusion.23
  254.0 1.6 fusion.27
  256.3 21.8 %all-to-all-done.2 = bf16[1,8,128,512]{3,2,0,1:T(8,128)(2,1)} async-done(((bf16[1,8,128,512]{3,2,0,1:T(8,128)(2,1)}), bf16[1,8,128,512]{3,2,0,1:T(8,128)(2,1)}, u32[]{:S(2)}, u32[]{:S(2)}) %all-to-all-start.2) | async-done | bytes 1048608 | tf_op jit(solution)/shard_map/all_to_all | solution.py:140
  278.0 3.3 %gather_fusion.2 = bf16[512,512]{1,0:T(8,128)(2,1)S(1)} fusion(bf16[1024,512]{1,0:T(8,128)(2,1)} %bitcast.25, s32[1024]{0:T(1024)S(1)} %pad_clamp_fusion), kind=kCustom, calls=%fused_computation.2 | custom fusion | bytes 1050624 | tf_op jit(solution)/shard_map/jit(_take)/gather | solution.py:143
  281.6 1.8 fusion.30
  283.4 3.4 %fusion.26 = bf16[256,512]{1,0:T(8,128)(2,1)} fusion(bf16[256,2048]{1,0:T(8,128)(2,1)} %all-gather.8.cloned.1.call-done, bf16[2048,512]{1,0:T(8,128)(2,1)} %param.27, f32[256,1,512]{2,1,0:T(1,128)} %fusion.30, bf16[256,512]{1,0:T(8,128)(2,1)S(1)} %copy-done.3), kind=kOutput, calls=%fused_computation.35 | convolution fusion | flops 537395200 | bytes 4194304 | tf_op jit(solution)/shard_map/dot_general | solution.py:138
  (82 shorter events, 7.2 us)
Async XLA Ops:
  6.5 234.7 %copy-start = (bf16[1,2048,512]{2,1,0:T(8,128)(2,1)S(1)}, bf16[1,2048,512]{2,1,0:T(8,128)(2,1)}, u32[]{:S(2)}) copy-start(bf16[1,2048,512]{2,1,0:T(8,128)(2,1)} %param.24) | copy-start | bytes 6291460
  7.8 5.5 %copy-start.2 = (bf16[2,256,256]{1,2,0:T(8,128)(2,1)}, bf16[2,256,256]{1,2,0:T(8,128)(2,1)S(1)}, u32[]{:S(2)}) copy-start(bf16[2,256,256]{1,2,0:T(8,128)(2,1)S(1)} %copy.63) | copy-start | bytes 786436
  7.8 10.9 %copy-start.4 = (bf16[256,256]{1,0:T(8,128)(2,1)S(1)}, bf16[256,256]{1,0:T(8,128)(2,1)}, u32[]{:S(2)}) copy-start(bf16[256,256]{1,0:T(8,128)(2,1)} %param.14) | copy-start | bytes 393220
  7.8 11.8 %collective-permute-start = (bf16[2,128,256]{1,2,0:T(8,128)(2,1)S(1)}, bf16[2,128,256]{1,2,0:T(8,128)(2,1)}, u32[]{:S(2)}, u32[]{:S(2)}) collective-permute-start(bf16[2,128,256]{1,2,0:T(8,128)(2,1)S(1)} %slice.34), channel_id=1, source_target_pairs={{0,4},{4,8},{8,12},{12,16},{16,20},{20,24},{24,28},{1,5},{5,9},{9,... | collective-permute-start | bytes 393224 | tf_op jit(solution)/shard_map/ppermute | solution.py:20
  13.3 29.4 %all-to-all-start = ((bf16[256,4,512]{0,2,1:T(8,128)(2,1)}), bf16[256,4,512]{0,2,1:T(8,128)(2,1)S(1)}, u32[]{:S(2)}, u32[]{:S(2)}) async-start(bf16[256,4,512]{0,2,1:T(8,128)(2,1)} %bitcast.91), calls=%async_computation | async-start | bytes 2097152 | tf_op jit(solution)/shard_map/all_to_all | solution.py:81
  17.8 54.0 %all-gather.6.cloned.1.call-start = ((), (), s32[]{:S(2)}) async-start(), calls=%async_computation.3 | async-start | bytes 1310720 | tf_op jit(solution)/shard_map/all_gather | solution.py:91
  22.0 5.6 %copy-start.6 = (pred[2,128,256]{1,2,0:T(8,128)(4,1)S(1)}, pred[2,128,256]{1,2,0:T(8,128)(4,1)}, u32[]{:S(2)}) copy-start(pred[2,128,256]{1,2,0:T(8,128)(4,1)} %broadcast_and_fusion) | copy-start | bytes 196612
  24.0 5.1 %copy-start.9 = (f32[4]{0:T(128)S(1)}, f32[4]{0:T(128)}, u32[]{:S(2)}) copy-start(f32[4]{0:T(128)} %param.16) | copy-start | bytes 52
  27.6 1.8 copy-start.5
  29.8 14.3 %copy-start.13 = (bf16[256,512]{1,0:T(8,128)(2,1)S(1)}, bf16[256,512]{1,0:T(8,128)(2,1)}, u32[]{:S(2)}) copy-start(bf16[256,512]{1,0:T(8,128)(2,1)} %param.18) | copy-start | bytes 786436
  42.7 4.0 %copy-start.7 = (s32[256,2]{0,1:T(2,128)S(1)}, s32[256,2]{0,1:T(2,128)}, u32[]{:S(2)}) copy-start(s32[256,2]{0,1:T(2,128)} %param.20) | copy-start | bytes 6148
  46.6 194.7 %all-gather.10.cloned.1.call-start = ((), (), s32[]{:S(2)}) async-start(), calls=%async_computation.5 | async-start | bytes 5242880 | tf_op jit(solution)/shard_map/all_gather | solution.py:133
  182.9 1.6 copy-start.10
  182.9 1.6 copy-start.14
  184.5 2.4 copy-start.11
  186.9 3.8 %copy-start.1 = (bf16[256,2048]{1,0:T(8,128)(2,1)S(1)}, bf16[256,2048]{1,0:T(8,128)(2,1)}, u32[]{:S(2)}) copy-start(bf16[256,2048]{1,0:T(8,128)(2,1)} %all-gather.6.cloned.1.call-done) | copy-start | bytes 3145732
  246.8 31.3 %all-to-all-start.2 = ((bf16[1,8,128,512]{3,2,0,1:T(8,128)(2,1)}), bf16[1,8,128,512]{3,2,0,1:T(8,128)(2,1)}, u32[]{:S(2)}, u32[]{:S(2)}) async-start(bf16[1,8,128,512]{3,2,0,1:T(8,128)(2,1)} %bitcast.93), calls=%async_computation.2 | async-start | bytes 2097152 | tf_op jit(solution)/shard_map/all_to_all | solution.py:140
  251.4 32.0 %all-gather.8.cloned.1.call-start = ((), (), s32[]{:S(2)}) async-start(), calls=%async_computation.4 | async-start | bytes 1310720 | tf_op jit(solution)/shard_map/all_gather | solution.py:134
  251.4 2.6 copy-start.12
  254.0 2.1 copy-start.8
  281.6 1.8 copy-start.3
Sparse Core Ops, SparseCore 0:
  46.7 25.0 all-gather.5
  190.8 50.3 all-gather.9
  255.8 26.7 all-gather.7
where the time goes:
time: 294 us; the launch traced here: 293 us
  blocking collectives  111 us (38%)
  waiting for transfers between devices  92.4 us (31%)
  local copies, waits for them, and re-layouts  30.1 us (10%)
  matrix products  25.3 us (9%)
  between operations  13.5 us (5%)
  starting transfers between devices  12.4 us (4%)
  other arithmetic  8.46 us (3%)
    all_to_all x1, blocking collectives, per_device(): lax.all_to_all(picked_rows.reshape(EXP_DEV, sp_count, capacity, stream_ro...  98.4 us
    all_gather x1, waiting for transfers between devices, per_device(): routed_piece = lax.all_gather(hidden, 'tp', axis=2, tiled=True)  50.3 us
    all_to_all x1, waiting for transfers between devices, per_device(): lax.all_to_all(outgoing, 'sp', split_axis=1, concat_axis=1, tiled=True)  21.8 us
    all_gather x1, waiting for transfers between devices, per_device(): stream_rows = lax.all_gather(stream_cols, 'tp', axis=1, tiled=True)  20.4 us
    all_gather x1, blocking collectives, per_device(): attended_all = lax.all_gather(attended_values, 'tp', axis=1, tiled=True)  12.7 us
    gather x1, local copies, waits for them, and re-layouts, per_device(): jnp.take(stream_rows, slot_owner, axis=0, mode='fill', fill_value=0)  10.2 us
  transfers between devices with their start and end apart: 6, of which 3 were waited for; matrix products, arithmetic and copies ran while one was open for 10% of the time, Pallas kernels for 0%

commit v1 on v0

--- a/solution.py
+++ b/solution.py
@@ -130,7 +130,12 @@
     shared_hidden = (jax.nn.silu(own_scale * shared_gate_sum) * (own_scale * shared_up_sum)).astype(
         jnp.bfloat16
     )
-    routed_piece = lax.all_gather(hidden, "tp", axis=2, tiled=True)
+    ring = [hidden]
+    for hop in range(3):
+        ring.append(lax.ppermute(ring[-1], "tp", [(dev, (dev + 1) % 4) for dev in range(4)]))
+    routed_piece = jnp.roll(
+        jnp.concatenate(ring[::-1], axis=2), (lax.axis_index("tp") + 1) * ring[0].shape[2], axis=2
+    )
     own_piece = lax.all_gather(shared_hidden[None], "tp", axis=2, tiled=True)
     expert_out = jnp.einsum(
         "erf,efd->erd", routed_piece, down_weight, preferred_element_type=jnp.float32

time: 294 us -> 323 us (1.099)
  waiting for transfers between devices: 92.4 us -> 113 us
  local copies, waits for them, and re-layouts: 30.1 us -> 38.1 us
    ppermute x0 -> x3, waiting for transfers between devices: none -> 71.8 us  [per_device(): lax.ppermute(ring[-1], 'tp', [(dev, (dev + 1) % 4) for dev in range(4)])]
    all_gather x1 -> x0, waiting for transfers between devices: 50.3 us -> none  [per_device(): routed_piece = lax.all_gather(hidden, 'tp', axis=2, tiled=True)]
    unnamed x36 -> x47, local copies, waits for them, and re-layouts: 5.35 us -> 12.7 us
  transfers between devices with their start and end apart: 6 -> 8, of which waited for: 3 -> 5; matrix products, arithmetic and copies ran while one was open for 10% -> 10% of each run, Pallas kernels for 0% -> 0%
where the time goes in v1:
time: 323 us; the launch traced here: 322 us
  waiting for transfers between devices  113 us (35%)
  blocking collectives  111 us (34%)
  local copies, waits for them, and re-layouts  38.1 us (12%)
  matrix products  23.2 us (7%)
  starting transfers between devices  14.3 us (4%)
  between operations  13.8 us (4%)
  other arithmetic  8.43 us (3%)
    all_to_all x1, blocking collectives, per_device(): lax.all_to_all(picked_rows.reshape(EXP_DEV, sp_count, capacity, stream_ro...  98.4 us
    ppermute x3, waiting for transfers between devices, per_device(): lax.ppermute(ring[-1], 'tp', [(dev, (dev + 1) % 4) for dev in range(4)])  71.8 us
    all_to_all x1, waiting for transfers between devices, per_device(): lax.all_to_all(outgoing, 'sp', split_axis=1, concat_axis=1, tiled=True)  21 us
    all_gather x1, waiting for transfers between devices, per_device(): stream_rows = lax.all_gather(stream_cols, 'tp', axis=1, tiled=True)  20.4 us
    all_gather x1, blocking collectives, per_device(): attended_all = lax.all_gather(attended_values, 'tp', axis=1, tiled=True)  12.8 us
    unnamed x47, local copies, waits for them, and re-layouts  12.7 us
    gather x1, local copies, waits for them, and re-layouts, per_device(): jnp.take(stream_rows, slot_owner, axis=0, mode='fill', fill_value=0)  10.2 us
  transfers between devices with their start and end apart: 8, of which 5 were waited for; matrix products, arithmetic and copies ran while one was open for 10% of the time, Pallas kernels for 0%

profile of v1, /device:TPU:0, one launch (start us, length us, event | category | flops | bytes accessed | tf_op | source)
XLA Modules:
  0.0 322.3 jit_solution(8702760240747145335)
XLA Ops:
  7.8 3.1 collective-permute-start
  10.9 2.3 copy.73
  13.1 4.5 %all-to-all-start = ((bf16[256,4,512]{0,2,1:T(8,128)(2,1)}), bf16[256,4,512]{0,2,1:T(8,128)(2,1)S(1)}, u32[]{:S(2)}, u32[]{:S(2)}) async-start(bf16[256,4,512]{0,2,1:T(8,128)(2,1)} %bitcast.99), calls=%async_computation | async-start | bytes 2097152 | tf_op jit(solution)/shard_map/all_to_all | solution.py:81
  20.5 1.4 gather_fusion
  27.5 1.4 fusion.56
  29.2 1.3 fusion.35
  30.7 12.8 %all_gather.9 = bf16[256,1024]{0,1:T(8,128)(2,1)} all-gather(bf16[256,256]{0,1:T(8,128)(2,1)S(1)} %bitcast.103), channel_id=1, replica_groups=mesh['sp'=8,'tp'=4] {'tp'}, dimensions={1}, use_global_device_ids=true | all-gather | bytes 655360 | tf_op jit(solution)/shard_map/all_gather | solution.py:79
  43.4 1.3 copy.74
  44.7 2.5 fusion.32
  49.6 2.4 scatter_custom_fusion
  52.1 20.4 %all-gather.4.cloned.1.call-done = bf16[256,2048]{1,0:T(8,128)(2,1)} async-done(((bf16[256,512]{1,0:T(8,128)(2,1)}), bf16[256,2048]{1,0:T(8,128)(2,1)}) %all-gather.4.cloned.1.call-update) | async-done | bytes 1048592 | tf_op jit(solution)/shard_map/all_gather | solution.py:91
  72.5 10.2 %gather_fusion.1 = bf16[1024,2048]{1,0:T(8,128)(2,1)} fusion(bf16[256,2048]{1,0:T(8,128)(2,1)} %all-gather.4.cloned.1.call-done, s32[1024]{0:T(1024)S(1)} %fusion.46), kind=kCustom, calls=%fused_computation.1 | custom fusion | bytes 8392704 | tf_op jit(solution)/shard_map/jit(_take)/gather | solution.py:112
  82.6 2.5 broadcast_select_fusion
  85.2 98.4 %all_to_all.25 = bf16[1,8,128,2048]{3,2,0,1:T(8,128)(2,1)S(1)} all-to-all(bf16[1,8,128,2048]{3,2,0,1:T(8,128)(2,1)S(1)} %broadcast_select_fusion), channel_id=1, replica_groups=mesh['sp'=8,'tp'=4] {'sp'}, dimensions={1} | all-to-all | bytes 8388608 | tf_op jit(solution)/shard_map/all_to_all | solution.py:113
  185.1 2.5 fusion.6
  187.7 2.8 fusion.23
  191.6 1.5 collective-permute-start.1
  193.0 24.0 %collective-permute-done.1 = bf16[1,1024,512]{1,2,0:T(8,128)(2,1)S(1)} collective-permute-done((bf16[1,1024,512]{1,2,0:T(8,128)(2,1)S(1)}, bf16[1,1024,512]{1,2,0:T(8,128)(2,1)S(1)}, u32[]{:S(2)}, u32[]{:S(2)}) %collective-permute-start.1) | collective-permute-done | bytes 1048608 | tf_op jit(solution)/shard_map/ppermute | solution.py:135
  218.6 24.1 %collective-permute-done.2 = bf16[1,1024,512]{1,2,0:T(8,128)(2,1)} collective-permute-done((bf16[1,1024,512]{1,2,0:T(8,128)(2,1)S(1)}, bf16[1,1024,512]{1,2,0:T(8,128)(2,1)}, u32[]{:S(2)}, u32[]{:S(2)}) %collective-permute-start.2) | collective-permute-done | bytes 1048608 | tf_op jit(solution)/shard_map/ppermute | solution.py:135
  243.0 23.7 %collective-permute-done.3 = bf16[1,1024,512]{1,2,0:T(8,128)(2,1)} collective-permute-done((bf16[1,1024,512]{1,2,0:T(8,128)(2,1)}, bf16[1,1024,512]{1,2,0:T(8,128)(2,1)}, u32[]{:S(2)}, u32[]{:S(2)}) %collective-permute-start.3) | collective-permute-done | bytes 1048608 | tf_op jit(solution)/shard_map/ppermute | solution.py:135
  266.7 1.3 constant_dynamic-update-slice_fusion.7
  268.0 1.3 constant_dynamic-update-slice_fusion.6
  269.5 1.3 constant_dynamic-update-slice_fusion.3
  270.8 1.3 constant_dynamic-update-slice_fusion.2
  272.2 3.4 %fusion.18 = bf16[1024,512]{1,0:T(8,128)(2,1)} fusion(bf16[1,2048,512]{2,1,0:T(8,128)(2,1)S(1)} %copy-done, bf16[1,1024,4096]{1,2,0:T(8,128)(2,1)S(1)} %constant_dynamic-update-slice_fusion, s32[]{:T(128)S(6)} %select_n.121), kind=kOutput, calls=%fused_computation.26 | convolution fusion | flops 2148007936 | bytes 7340036 | tf_op jit(solution)/shard_map/erf,efd->erd/dot_general | solution.py:140
  275.6 4.4 %all-to-all-start.2 = ((bf16[1,8,128,512]{3,2,0,1:T(8,128)(2,1)}), bf16[1,8,128,512]{3,2,0,1:T(8,128)(2,1)}, u32[]{:S(2)}, u32[]{:S(2)}) async-start(bf16[1,8,128,512]{3,2,0,1:T(8,128)(2,1)} %bitcast.101), calls=%async_computation.2 | async-start | bytes 2097152 | tf_op jit(solution)/shard_map/all_to_all | solution.py:145
  280.3 2.6 fusion.30
  282.9 1.6 fusion.34
  285.7 21.0 %all-to-all-done.2 = bf16[1,8,128,512]{3,2,0,1:T(8,128)(2,1)} async-done(((bf16[1,8,128,512]{3,2,0,1:T(8,128)(2,1)}), bf16[1,8,128,512]{3,2,0,1:T(8,128)(2,1)}, u32[]{:S(2)}, u32[]{:S(2)}) %all-to-all-start.2) | async-done | bytes 1048608 | tf_op jit(solution)/shard_map/all_to_all | solution.py:145
  306.7 3.4 %gather_fusion.2 = bf16[512,512]{1,0:T(8,128)(2,1)S(1)} fusion(bf16[1024,512]{1,0:T(8,128)(2,1)} %bitcast.27, s32[1024]{0:T(1024)S(1)} %pad_clamp_fusion), kind=kCustom, calls=%fused_computation.2 | custom fusion | bytes 1050624 | tf_op jit(solution)/shard_map/jit(_take)/gather | solution.py:148
  310.3 1.8 fusion.37
  312.1 3.3 %fusion.33 = bf16[256,512]{1,0:T(8,128)(2,1)} fusion(bf16[256,2048]{1,0:T(8,128)(2,1)} %all-gather.6.cloned.1.call-done, bf16[2048,512]{1,0:T(8,128)(2,1)} %param.27, f32[256,1,512]{2,1,0:T(1,128)S(1)} %fusion.37, bf16[256,512]{1,0:T(8,128)(2,1)S(1)} %copy-done.7), kind=kOutput, calls=%fused_computation.38 | convolution fusion | flops 537395200 | bytes 4194304 | tf_op jit(solution)/shard_map/dot_general | solution.py:143
  (97 shorter events, 18.8 us)
Async XLA Ops:
  6.5 265.7 %copy-start = (bf16[1,2048,512]{2,1,0:T(8,128)(2,1)S(1)}, bf16[1,2048,512]{2,1,0:T(8,128)(2,1)}, u32[]{:S(2)}) copy-start(bf16[1,2048,512]{2,1,0:T(8,128)(2,1)} %param.24) | copy-start | bytes 6291460
  6.5 12.1 %copy-start.8 = (bf16[256,256]{1,0:T(8,128)(2,1)S(1)}, bf16[256,256]{1,0:T(8,128)(2,1)}, u32[]{:S(2)}) copy-start(bf16[256,256]{1,0:T(8,128)(2,1)} %param.14) | copy-start | bytes 393220
  7.8 5.3 %copy-start.6 = (bf16[2,256,256]{1,2,0:T(8,128)(2,1)}, bf16[2,256,256]{1,2,0:T(8,128)(2,1)S(1)}, u32[]{:S(2)}) copy-start(bf16[2,256,256]{1,2,0:T(8,128)(2,1)S(1)} %copy.63) | copy-start | bytes 786436
  7.8 11.7 %collective-permute-start = (bf16[2,128,256]{1,2,0:T(8,128)(2,1)S(1)}, bf16[2,128,256]{1,2,0:T(8,128)(2,1)}, u32[]{:S(2)}, u32[]{:S(2)}) collective-permute-start(bf16[2,128,256]{1,2,0:T(8,128)(2,1)S(1)} %slice.34), channel_id=1, source_target_pairs={{0,4},{4,8},{8,12},{12,16},{16,20},{20,24},{24,28},{1,5},{5,9},{9,... | collective-permute-start | bytes 393224 | tf_op jit(solution)/shard_map/ppermute | solution.py:20
  13.1 30.3 %all-to-all-start = ((bf16[256,4,512]{0,2,1:T(8,128)(2,1)}), bf16[256,4,512]{0,2,1:T(8,128)(2,1)S(1)}, u32[]{:S(2)}, u32[]{:S(2)}) async-start(bf16[256,4,512]{0,2,1:T(8,128)(2,1)} %bitcast.99), calls=%async_computation | async-start | bytes 2097152 | tf_op jit(solution)/shard_map/all_to_all | solution.py:81
  17.7 54.8 %all-gather.4.cloned.1.call-start = ((), (), s32[]{:S(2)}) async-start(), calls=%async_computation.3 | async-start | bytes 1310720 | tf_op jit(solution)/shard_map/all_gather | solution.py:91
  18.6 10.3 %copy-start.11 = (f32[4]{0:T(128)S(1)}, f32[4]{0:T(128)}, u32[]{:S(2)}) copy-start(f32[4]{0:T(128)} %param.16) | copy-start | bytes 52
  28.9 15.8 %copy-start.15 = (bf16[256,512]{1,0:T(8,128)(2,1)S(1)}, bf16[256,512]{1,0:T(8,128)(2,1)}, u32[]{:S(2)}) copy-start(bf16[256,512]{1,0:T(8,128)(2,1)} %param.18) | copy-start | bytes 786436
  29.2 18.1 %copy-start.9 = (s32[256,2]{0,1:T(2,128)S(1)}, s32[256,2]{0,1:T(2,128)}, u32[]{:S(2)}) copy-start(s32[256,2]{0,1:T(2,128)} %param.20) | copy-start | bytes 6148
  183.5 1.6 copy-start.12
  183.6 1.6 copy-start.16
  185.1 2.5 copy-start.13
  187.7 55.0 %copy-start.1 = (bf16[256,2048]{1,0:T(8,128)(2,1)S(1)}, bf16[256,2048]{1,0:T(8,128)(2,1)}, u32[]{:S(2)}) copy-start(bf16[256,2048]{1,0:T(8,128)(2,1)} %all-gather.4.cloned.1.call-done) | copy-start | bytes 3145732
  190.5 1.0 copy-start.2
  191.6 25.4 %collective-permute-start.1 = (bf16[1,1024,512]{1,2,0:T(8,128)(2,1)S(1)}, bf16[1,1024,512]{1,2,0:T(8,128)(2,1)S(1)}, u32[]{:S(2)}, u32[]{:S(2)}) collective-permute-start(bf16[1,1024,512]{1,2,0:T(8,128)(2,1)S(1)} %fusion.23), channel_id=1, source_target_pairs={{0,1},{1,2},{2,3},{3,0},{4,5},{5,6},{6,7},{7,4},{8,9},{9,10},{10,1... | collective-permute-start | bytes 3145736 | tf_op jit(solution)/shard_map/ppermute | solution.py:135
  217.0 1.0 copy-start.4
  218.0 24.7 %collective-permute-start.2 = (bf16[1,1024,512]{1,2,0:T(8,128)(2,1)S(1)}, bf16[1,1024,512]{1,2,0:T(8,128)(2,1)}, u32[]{:S(2)}, u32[]{:S(2)}) collective-permute-start(bf16[1,1024,512]{1,2,0:T(8,128)(2,1)S(1)} %collective-permute-done.1), channel_id=1, source_target_pairs={{0,1},{1,2},{2,3},{3,0},{4,5},{5,6},{6,7},{7,4},{8,9},{9,10},{10,1... | collective-permute-start | bytes 3145736 | tf_op jit(solution)/shard_map/ppermute | solution.py:135
  242.7 24.0 %collective-permute-start.3 = (bf16[1,1024,512]{1,2,0:T(8,128)(2,1)}, bf16[1,1024,512]{1,2,0:T(8,128)(2,1)}, u32[]{:S(2)}, u32[]{:S(2)}) collective-permute-start(bf16[1,1024,512]{1,2,0:T(8,128)(2,1)} %collective-permute-done.2), channel_id=1, source_target_pairs={{0,1},{1,2},{2,3},{3,0},{4,5},{5,6},{6,7},{7,4},{8,9},{9,10},{10,1... | collective-permute-start | bytes 3145736 | tf_op jit(solution)/shard_map/ppermute | solution.py:135
  242.7 26.6 %copy-start.5 = (bf16[1,1024,512]{1,2,0:T(8,128)(2,1)S(1)}, bf16[1,1024,512]{1,2,0:T(8,128)(2,1)}, u32[]{:S(2)}) copy-start(bf16[1,1024,512]{1,2,0:T(8,128)(2,1)} %copy-done.4) | copy-start | bytes 3145732
  242.7 26.7 %copy-start.3 = (bf16[1,1024,512]{1,2,0:T(8,128)(2,1)S(1)}, bf16[1,1024,512]{1,2,0:T(8,128)(2,1)}, u32[]{:S(2)}) copy-start(bf16[1,1024,512]{1,2,0:T(8,128)(2,1)} %copy-done.2) | copy-start | bytes 3145732
  275.6 31.1 %all-to-all-start.2 = ((bf16[1,8,128,512]{3,2,0,1:T(8,128)(2,1)}), bf16[1,8,128,512]{3,2,0,1:T(8,128)(2,1)}, u32[]{:S(2)}, u32[]{:S(2)}) async-start(bf16[1,8,128,512]{3,2,0,1:T(8,128)(2,1)} %bitcast.101), calls=%async_computation.2 | async-start | bytes 2097152 | tf_op jit(solution)/shard_map/all_to_all | solution.py:145
  280.0 32.1 %all-gather.6.cloned.1.call-start = ((), (), s32[]{:S(2)}) async-start(), calls=%async_computation.4 | async-start | bytes 1310720 | tf_op jit(solution)/shard_map/all_gather | solution.py:139
  280.3 2.6 copy-start.14
  282.8 2.6 copy-start.10
  306.7 5.4 %copy-start.7 = (bf16[256,512]{1,0:T(8,128)(2,1)S(1)}, bf16[256,512]{1,0:T(8,128)(2,1)}, u32[]{:S(2)}) copy-start(bf16[256,512]{1,0:T(8,128)(2,1)} %fusion.32) | copy-start | bytes 786436
Sparse Core Ops, SparseCore 0:
  47.4 24.9 all-gather.3
  284.6 26.5 all-gather.5
